TPU v7x, 32 devices: a whole 2x2x4 slice. The times are simulated.
32 devices in a mesh: sp: 4 (over z), fs: 4 (over y, x), tp: 2 (over core).
Axes of the slice: x: 2, y: 2, z: 4, core: 2. Of those that a mesh axis runs over, the one named last changes fastest.
Arguments:
- tokens: bfloat16 [4, 1024, 2048], P('fs', 'sp', 'tp'), may hold values from -6 to 6
- norm_gain: float32 [2048], replicated, may hold values from 0.1 to 1.9
- w_query: bfloat16 [2048, 1024], P(('sp', 'fs'), 'tp'), may hold values from -0.125 to 0.125
- forget_weight: bfloat16 [2048, 1024], P(('sp', 'fs'), 'tp'), may hold values from -0.125 to 0.125
- w_input: bfloat16 [2048, 1024], P(('sp', 'fs'), 'tp'), may hold values from -8 to 8
- w_outgate: bfloat16 [2048, 1024], P(('sp', 'fs'), 'tp'), may hold values from -0.125 to 0.125
- w_pool: bfloat16 [2048, 1024], P(('sp', 'fs'), 'tp'), may hold values from -0.125 to 0.125
- forget_gap: float32 [1024], P('tp'), may hold values from 0 to 0.07
- extra_decay: float32 [4, 1024, 8], P('fs', 'sp', 'tp'), may hold values from -0.61 to 0
- rec_gain: float32 [1024], P('tp'), may hold values from 0.1 to 1.9
- group_weight: bfloat16 [4, 256, 256], replicated, may hold values from -0.375 to 0.375
- pool_gain: float32 [1024], P('tp'), may hold values from 0.1 to 1.9
- recurrent_output_weight: bfloat16 [1024, 2048], P('tp', ('sp', 'fs')), may hold values from -0.1875 to 0.1875
- w_out_pool: bfloat16 [1024, 2048], P('tp', ('sp', 'fs')), may hold values from -0.1875 to 0.1875
Outputs:
- mixed_out: bfloat16 [4, 1024, 2048], P('fs', ('sp', 'tp'))
All inputs are finite; a program needn't handle non-finite values.
Results may differ from a plain program's by a relative error of at most 0.011.
Values may be sent and summed in bfloat16 or wider, within the bound.
A program may use at most 64 MiB of HBM per device.

v0:
```python
import jax
import jax.numpy as jnp
from jax import lax
from jax.sharding import PartitionSpec as P

HEAD_DIM = 128
D_HGRN = 1024
POOL_GROUPS = 4
GROUP_DIM = 256
BLOCK = 64
EPS = 1e-06
HIGH = lax.Precision.HIGHEST


def carried_in(x, axis, join, neutral):
    place = lax.axis_index(axis)
    gathered = jax.tree.map(
        lambda a, kind: lax.all_gather(a.astype(kind), axis), x, (jnp.bfloat16, jnp.bfloat16)
    )
    state = jax.tree.map(lambda a, e: jnp.zeros_like(a) + jnp.asarray(e, a.dtype), x, neutral)

    def one(lap, state):
        return join(
            state,
            jax.tree.map(
                lambda a, own: lax.dynamic_index_in_dim(a, lap, 0, False).astype(own.dtype),
                gathered,
                x,
            ),
        )

    return lax.fori_loop(0, place, one, state)


def shifted(x, axis, by):
    peers = lax.axis_size(axis)
    pairs = [(i, i + by) for i in range(peers) if 0 <= i + by < peers]
    return lax.ppermute(x, axis, pairs)


def local_recurrence(queries, input_gate, values, log_forget):
    tok_rows, head_count = (queries.shape[0], queries.shape[1])
    block_count = tok_rows // BLOCK
    q_blk, k_blk, v_blk, g_blk = (
        arr.reshape(block_count, BLOCK, head_count, HEAD_DIM)
        for arr in (queries, input_gate, values, log_forget)
    )
    within = jnp.cumsum(g_blk, axis=1)
    block_end = within[:, -1]
    q_up = q_blk * jnp.exp(within)
    k_down = k_blk * jnp.exp(-within)
    causal = jnp.tril(jnp.ones((BLOCK, BLOCK), jnp.bool_))
    scores = jnp.einsum("nthd,nshd->nhts", q_up, k_down, precision=HIGH)
    scores = jnp.where(causal, scores, 0.0)
    inner_out = jnp.einsum("nhts,nshe->nthe", scores, v_blk, precision=HIGH)
    updates = jnp.einsum(
        "nshd,nshe->nhde", k_blk * jnp.exp(block_end[:, None] - within), v_blk, precision=HIGH
    )
    decays = jnp.exp(block_end)

    def carry_step(carried_state, step_inputs):
        current_shrink_factor, update_now = step_inputs
        return (current_shrink_factor[:, :, None] * carried_state + update_now, carried_state)

    zero_state = jnp.zeros((head_count, HEAD_DIM, HEAD_DIM), jnp.float32)
    final_state, incoming = lax.scan(carry_step, zero_state, (decays, updates))
    local_out = inner_out + jnp.einsum("nthd,nhde->nthe", q_up, incoming, precision=HIGH)
    offsets = jnp.cumsum(block_end, axis=0) - block_end
    total_log = jnp.sum(block_end, axis=0)
    query_dev = q_up * jnp.exp(offsets[:, None])
    return (local_out, final_state, total_log, query_dev)


def combine_states(earlier, later):
    decay_early, state_early = earlier
    decay_late, state_late = later
    return (decay_early * decay_late, decay_late[:, :, None] * state_early + state_late)


def body(
    tokens,
    norm_gain,
    w_query,
    forget_weight,
    w_input,
    w_outgate,
    w_pool,
    forget_gap,
    extra_decay,
    rec_gain,
    group_weight,
    pool_gain,
    recurrent_output_weight,
    w_out_pool,
):
    gathered = lax.all_gather(tokens[0], "tp", axis=1, tiled=True)
    features_f = gathered.astype(jnp.float32)
    token_scale = lax.rsqrt(jnp.mean(features_f * features_f, axis=-1, keepdims=True) + EPS)
    normed = (features_f * token_scale * norm_gain).astype(jnp.bfloat16)
    tok_rows = normed.shape[0]
    width_dev = w_query.shape[1]
    pool_dev = w_pool.shape[1]
    near_rows = (
        lax.all_gather(w_query, "fs", axis=0, tiled=True),
        lax.all_gather(forget_weight, "fs", axis=0, tiled=True),
        lax.all_gather(w_input, "fs", axis=0, tiled=True),
        lax.all_gather(w_outgate, "fs", axis=0, tiled=True),
        lax.all_gather(w_pool, "fs", axis=0, tiled=True),
    )
    full_rows = (
        lax.all_gather(near_rows[0], "sp", axis=0, tiled=True),
        lax.all_gather(near_rows[1], "sp", axis=0, tiled=True),
        lax.all_gather(near_rows[2], "sp", axis=0, tiled=True),
        lax.all_gather(near_rows[3], "sp", axis=0, tiled=True),
        lax.all_gather(near_rows[4], "sp", axis=0, tiled=True),
    )
    z_query, z_forget, z_input, z_outgate, z_pool = (
        jnp.dot(normed, matrix, preferred_element_type=jnp.float32).astype(jnp.bfloat16)
        for matrix in full_rows
    )
    heads_dev = width_dev // HEAD_DIM
    input_gate = forget_gap * jax.nn.sigmoid(-z_forget.astype(jnp.float32))
    log_forget = (
        jnp.log1p(-input_gate).reshape(tok_rows, heads_dev, HEAD_DIM) + extra_decay[0][:, :, None]
    )
    queries = jax.nn.silu(z_query.astype(jnp.float32)).reshape(tok_rows, heads_dev, HEAD_DIM)
    values = z_input.astype(jnp.float32).reshape(tok_rows, heads_dev, HEAD_DIM)
    local_out, end_state, total_log, query_dev = local_recurrence(
        queries, input_gate.reshape(tok_rows, heads_dev, HEAD_DIM), values, log_forget
    )
    identity = (jnp.ones_like(total_log), jnp.zeros_like(end_state))
    scanned = carried_in((jnp.exp(total_log), end_state), "sp", combine_states, identity)
    incoming = scanned[1]
    carried = jnp.einsum("nthd,hde->nthe", query_dev, incoming, precision=HIGH)
    recurrent = (local_out + carried).reshape(tok_rows, width_dev)
    square_sum = lax.psum(jnp.sum(recurrent * recurrent, axis=1), "tp")
    rec_scale = lax.rsqrt(square_sum / D_HGRN + EPS)[:, None]
    recurrent_output = (
        recurrent * rec_scale * rec_gain * jax.nn.silu(z_outgate.astype(jnp.float32))
    ).astype(jnp.bfloat16)
    reach_rows = 2**POOL_GROUPS
    rim_rows = shifted(z_pool[tok_rows - reach_rows :], "sp", 1)
    extended = jnp.concatenate([rim_rows, z_pool], axis=0).astype(jnp.float32)
    running = extended
    window_sums = []
    for level_idx in range(POOL_GROUPS):
        stride = 2**level_idx
        running = running[stride:] + running[:-stride]
        window_sums.append(running[running.shape[0] - tok_rows :])
    groups_dev = pool_dev // GROUP_DIM
    stacked = jnp.stack(window_sums).reshape(POOL_GROUPS, tok_rows, groups_dev, GROUP_DIM)
    group_ids = lax.axis_index("tp") * groups_dev + jnp.arange(groups_dev, dtype=jnp.int32)
    chosen = jnp.arange(POOL_GROUPS, dtype=jnp.int32)[:, None] == group_ids[None, :]
    window_total = jnp.sum(jnp.where(chosen[:, None, :, None], stacked, 0.0), axis=0)
    symbol_indices = lax.axis_index("sp") * tok_rows + jnp.arange(tok_rows, dtype=jnp.int32)
    window_len = jnp.left_shift(jnp.int32(2), group_ids)
    counts_here = jnp.minimum(symbol_indices[:, None] + 1, window_len[None, :]).astype(jnp.float32)
    pooled = (
        window_total / counts_here[:, :, None]
        - z_pool.astype(jnp.float32).reshape(tok_rows, groups_dev, GROUP_DIM)
    ).astype(jnp.bfloat16)
    local_weight = lax.dynamic_slice_in_dim(
        group_weight, lax.axis_index("tp") * groups_dev, groups_dev, 0
    )
    mapped = jnp.einsum("tcd,cde->tce", pooled, local_weight, preferred_element_type=jnp.float32)
    pool_out = (mapped.reshape(tok_rows, pool_dev) * pool_gain).astype(jnp.bfloat16)
    rec_columns, pool_columns = (
        lax.all_gather(recurrent_output_weight, ("sp", "fs"), axis=1, tiled=True),
        lax.all_gather(w_out_pool, ("sp", "fs"), axis=1, tiled=True),
    )
    mixed = lax.psum_scatter(
        (
            jnp.dot(recurrent_output, rec_columns, preferred_element_type=jnp.float32)
            + jnp.dot(pool_out, pool_columns, preferred_element_type=jnp.float32)
        ).astype(jnp.bfloat16),
        "tp",
        scatter_dimension=0,
        tiled=True,
    )
    return mixed[None]


def solution(mesh):
    placed = (
        P("fs", "sp", "tp"),
        P(),
        P(("sp", "fs"), "tp"),
        P(("sp", "fs"), "tp"),
        P(("sp", "fs"), "tp"),
        P(("sp", "fs"), "tp"),
        P(("sp", "fs"), "tp"),
        P("tp"),
        P("fs", "sp", "tp"),
        P("tp"),
        P(),
        P("tp"),
        P("tp", ("sp", "fs")),
        P("tp", ("sp", "fs")),
    )
    return jax.shard_map(
        body, mesh=mesh, in_specs=placed, out_specs=P("fs", ("sp", "tp"), None), check_vma=False
    )
```

profile of v0, /device:TPU:0, one launch (start us, length us, event | category | flops | bytes accessed | tf_op | source)
XLA Modules:
  0.0 406.3 jit_solution(6593802053966810310)
XLA Ops:
  6.5 0.7 all-gather.27.cloned.1.call-update
  7.3 13.2 %all_gather.54 = bf16[512,512]{1,0:T(8,128)(2,1)} all-gather(bf16[128,512]{1,0:T(8,128)(2,1)} %param.21), channel_id=1, replica_groups=mesh['sp'=4,'fs'=4,'tp'=2] {'fs'}, dimensions={0}, use_global_device_ids=true | all-gather | bytes 655360 | tf_op jit(solution)/shard_map/all_gather | solution.py:105
  20.6 11.4 %all_gather.62 = bf16[512,512]{1,0:T(8,128)(2,1)} all-gather(bf16[128,512]{1,0:T(8,128)(2,1)} %param.24), channel_id=1, replica_groups=mesh['sp'=4,'fs'=4,'tp'=2] {'fs'}, dimensions={0}, use_global_device_ids=true | all-gather | bytes 655360 | tf_op jit(solution)/shard_map/all_gather | solution.py:108
  32.1 10.5 %all_gather.52 = bf16[512,512]{1,0:T(8,128)(2,1)} all-gather(bf16[128,512]{1,0:T(8,128)(2,1)S(1)} %copy-done.6), channel_id=1, replica_groups=mesh['sp'=4,'fs'=4,'tp'=2] {'fs'}, dimensions={0}, use_global_device_ids=true | all-gather | bytes 655360 | tf_op jit(solution)/shard_map/all_gather | solution.py:104
  42.7 10.3 %all_gather.50 = bf16[512,512]{1,0:T(8,128)(2,1)} all-gather(bf16[128,512]{1,0:T(8,128)(2,1)S(1)} %copy-done.7), channel_id=1, replica_groups=mesh['sp'=4,'fs'=4,'tp'=2] {'fs'}, dimensions={0}, use_global_device_ids=true | all-gather | bytes 655360 | tf_op jit(solution)/shard_map/all_gather | solution.py:106
  53.1 10.0 %all_gather.59 = bf16[512,512]{1,0:T(8,128)(2,1)} all-gather(bf16[128,512]{1,0:T(8,128)(2,1)S(1)} %copy-done.8), channel_id=1, replica_groups=mesh['sp'=4,'fs'=4,'tp'=2] {'fs'}, dimensions={0}, use_global_device_ids=true | all-gather | bytes 655360 | tf_op jit(solution)/shard_map/all_gather | solution.py:107
  63.2 0.7 all-gather.21.cloned.1.call-update
  63.9 0.7 all-gather.25.cloned.1.call-update
  65.7 1.5 fusion.1
  67.2 1.9 all-gather.17.cloned.1.call-done
  69.1 2.9 negate_log-plus-one_fusion
  72.5 1.2 slice_bitcast_fusion
  73.7 0.6 fusion.15
  74.4 40.8 %all-gather.23.cloned.1.call-done = bf16[2048,512]{1,0:T(8,128)(2,1)} async-done(((bf16[512,512]{1,0:T(8,128)(2,1)}), bf16[2048,512]{1,0:T(8,128)(2,1)}) %all-gather.23.cloned.1.call-update) | async-done | bytes 2097168 | tf_op jit(solution)/shard_map/all_gather | solution.py:115
  115.2 2.7 convolution_convert_fusion
  117.9 0.6 slice.57
  118.5 2.7 collective-permute-start
  121.1 1.0 reshape_reshape.11
  122.1 39.0 %all-gather.15.cloned.1.call-done = bf16[2048,512]{1,0:T(8,128)(2,1)} async-done(((bf16[512,512]{1,0:T(8,128)(2,1)}), bf16[2048,512]{1,0:T(8,128)(2,1)}) %all-gather.15.cloned.1.call-update) | async-done | bytes 2097168 | tf_op jit(solution)/shard_map/all_gather | solution.py:111
  161.1 2.4 divide_multiply_fusion
  163.5 1.1 reshape_reshape.10
  164.6 42.4 %all-gather.13.cloned.1.call-done = bf16[2048,512]{1,0:T(8,128)(2,1)} async-done(((bf16[512,512]{1,0:T(8,128)(2,1)}), bf16[2048,512]{1,0:T(8,128)(2,1)}) %all-gather.13.cloned.1.call-update) | async-done | bytes 2097168 | tf_op jit(solution)/shard_map/all_gather | solution.py:113
  207.0 2.3 convolution_convert_fusion.4
  209.4 1.7 exponential_multiply_fusion.1
  211.1 1.0 convolution_select_fusion
  212.1 1.2 fusion.39
  213.3 1.0 fusion.21
  214.3 3.7 while.26
  214.3 0.7 bitcast_dynamic-update-slice_fusion.2
  215.2 0.7 bitcast_dynamic-update-slice_fusion.2
  216.2 0.7 bitcast_dynamic-update-slice_fusion.2
  217.1 0.7 bitcast_dynamic-update-slice_fusion.2
  218.0 21.9 %all-gather.2 = bf16[16,128,128]{2,1,0:T(8,128)(2,1)S(1)} all-gather(bf16[4,128,128]{2,1,0:T(8,128)(2,1)S(1)} %convert_element_type.97), channel_id=4, replica_groups=mesh['sp'=4,'fs'=4,'tp'=2] {'sp'}, dimensions={0}, use_global_device_ids=true | all-gather | bytes 655360 | tf_op jit(solution)/shard_map/all_gather | solution.py:18
  240.0 10.1 %all-gather.3 = bf16[4,4,128]{2,1,0:T(4,128)(2,1)S(1)} all-gather(bf16[1,4,128]{2,1,0:T(4,128)(2,1)S(1)} %fusion.42), channel_id=3, replica_groups=mesh['sp'=4,'fs'=4,'tp'=2] {'sp'}, dimensions={0}, use_global_device_ids=true | all-gather | bytes 5120 | tf_op jit(solution)/shard_map/all_gather | solution.py:18
  250.1 0.6 convolution_bitcast_fusion
  251.1 2.3 multiply_reduce_fusion
  253.6 2.6 psum.7
  256.5 1.1 copy.43
  257.7 0.8 maximum_convert_fusion
  259.1 1.1 stack.18
  260.3 1.1 stack.17
  261.4 1.1 stack.16
  262.9 2.6 fusion.4
  266.4 59.5 %all-gather.21.cloned.1.call-done = bf16[512,2048]{1,0:T(8,128)(2,1)} async-done(((bf16[512,128]{1,0:T(8,128)(2,1)}), bf16[512,2048]{1,0:T(8,128)(2,1)}) %all-gather.21.cloned.1.call-update) | async-done | bytes 2097168 | tf_op jit(solution)/shard_map/all_gather | solution.py:168
  325.9 4.0 fusion.24
  329.9 59.8 %all-gather.25.cloned.1.call-done = bf16[512,2048]{1,0:T(8,128)(2,1)} async-done(((bf16[512,128]{1,0:T(8,128)(2,1)}), bf16[512,2048]{1,0:T(8,128)(2,1)}) %all-gather.25.cloned.1.call-update) | async-done | bytes 2097168 | tf_op jit(solution)/shard_map/all_gather | solution.py:169
  389.7 3.3 fusion
  393.1 6.7 %reduce-scatter.2.cloned.1.call-done = bf16[128,2048]{1,0:T(8,128)(2,1)} async-done(((bf16[256,2048]{1,0:T(8,128)(2,1)}), bf16[128,2048]{1,0:T(8,128)(2,1)}) %reduce-scatter.2.cloned.1.call-update) | async-done | bytes 524304 | tf_op jit(solution)/shard_map/reduce_scatter | solution.py:171
  (95 shorter events, 5.4 us)
Async XLA Ops:
  6.5 259.4 %copy-start = (bf16[4,256,256]{2,1,0:T(8,128)(2,1)S(1)}, bf16[4,256,256]{2,1,0:T(8,128)(2,1)}, u32[]{:S(2)}) copy-start(bf16[4,256,256]{2,1,0:T(8,128)(2,1)} %param.28) | copy-start | bytes 1572868
  6.5 25.5 %copy-start.6 = (bf16[128,512]{1,0:T(8,128)(2,1)S(1)}, bf16[128,512]{1,0:T(8,128)(2,1)}, u32[]{:S(2)}) copy-start(bf16[128,512]{1,0:T(8,128)(2,1)} %param.20) | copy-start | bytes 393220
  6.5 36.1 %copy-start.7 = (bf16[128,512]{1,0:T(8,128)(2,1)S(1)}, bf16[128,512]{1,0:T(8,128)(2,1)}, u32[]{:S(2)}) copy-start(bf16[128,512]{1,0:T(8,128)(2,1)} %param.22) | copy-start | bytes 393220
  6.5 59.1 %all-gather.27.cloned.1.call-start = ((), (), s32[]{:S(2)}) async-start(), calls=%async_computation.9 | async-start | bytes 1572864 | tf_op jit(solution)/shard_map/all_gather | solution.py:96
  7.3 61.8 %all-gather.17.cloned.1.call-start = ((), (), s32[]{:S(2)}) async-start(), calls=%async_computation.3 | async-start | bytes 2621440 | tf_op jit(solution)/shard_map/all_gather | solution.py:112
  20.5 32.6 %copy-start.8 = (bf16[128,512]{1,0:T(8,128)(2,1)S(1)}, bf16[128,512]{1,0:T(8,128)(2,1)}, u32[]{:S(2)}) copy-start(bf16[128,512]{1,0:T(8,128)(2,1)} %param.23) | copy-start | bytes 393220
  20.5 94.7 %all-gather.23.cloned.1.call-start = ((), (), s32[]{:S(2)}) async-start(), calls=%async_computation.6 | async-start | bytes 2621440 | tf_op jit(solution)/shard_map/all_gather | solution.py:115
  32.0 33.5 %copy-start.10 = (f32[1,256,4]{1,2,0:T(4,128)S(1)}, f32[1,256,4]{1,2,0:T(4,128)}, u32[]{:S(2)}) copy-start(f32[1,256,4]{1,2,0:T(4,128)} %param.26) | copy-start | bytes 12292
  32.0 129.1 %all-gather.15.cloned.1.call-start = ((), (), s32[]{:S(2)}) async-start(), calls=%async_computation.2 | async-start | bytes 2621440 | tf_op jit(solution)/shard_map/all_gather | solution.py:111
  42.6 26.5 %copy-start.15 = (f32[2048]{0:T(1024)S(1)}, f32[2048]{0:T(1024)}, u32[]{:S(2)}) copy-start(f32[2048]{0:T(1024)} %param.19) | copy-start | bytes 24580
  42.6 26.5 %copy-start.17 = (f32[512]{0:T(512)S(1)}, f32[512]{0:T(512)}, u32[]{:S(2)}) copy-start(f32[512]{0:T(512)} %param.25) | copy-start | bytes 6148
  42.6 164.4 %all-gather.13.cloned.1.call-start = ((), (), s32[]{:S(2)}) async-start(), calls=%async_computation.1 | async-start | bytes 2621440 | tf_op jit(solution)/shard_map/all_gather | solution.py:113
  53.1 213.4 %all-gather.19.cloned.1.call-start = ((), (), s32[]{:S(2)}) async-start(), calls=%async_computation.4 | async-start | bytes 2621440 | tf_op jit(solution)/shard_map/all_gather | solution.py:114
  63.1 262.7 %all-gather.21.cloned.1.call-start = ((), (), s32[]{:S(2)}) async-start(), calls=%async_computation.5 | async-start | bytes 2228224 | tf_op jit(solution)/shard_map/all_gather | solution.py:168
  63.9 325.9 %all-gather.25.cloned.1.call-start = ((), (), s32[]{:S(2)}) async-start(), calls=%async_computation.7 | async-start | bytes 2228224 | tf_op jit(solution)/shard_map/all_gather | solution.py:169
  64.6 335.2 %reduce-scatter.2.cloned.1.call-start = ((), (), s32[]{:S(2)}) async-start(), calls=%async_computation.8 | async-start | bytes 1572864 | tf_op jit(solution)/shard_map/reduce_scatter | solution.py:171
  67.2 139.8 %copy-start.12 = (f32[256]{0:T(256)}, f32[256]{0:T(256)S(1)}, u32[]{:S(2)}) copy-start(f32[256]{0:T(256)S(1)} %add_rsqrt_fusion.1) | copy-start | bytes 3076
  74.3 86.7 %copy-start.4 = (bf16[1,256,2048]{2,1,0:T(8,128)(2,1)S(1)}, bf16[1,256,2048]{2,1,0:T(8,128)(2,1)}, u32[]{:S(2)}) copy-start(bf16[1,256,2048]{2,1,0:T(8,128)(2,1)} %all-gather.27.cloned.1.call-done) | copy-start | bytes 3145732
  118.5 139.2 %collective-permute-start = (bf16[16,512]{1,0:T(8,128)(2,1)}, bf16[16,512]{1,0:T(8,128)(2,1)}, u32[]{:S(2)}, u32[]{:S(2)}) collective-permute-start(bf16[16,512]{1,0:T(8,128)(2,1)} %slice.57), channel_id=1, source_target_pairs={{0,8},{8,16},{16,24},{1,9},{9,17},{17,25},{2,10},{10,18},{18,26},{... | collective-permute-start | bytes 49160 | tf_op jit(solution)/shard_map/ppermute | solution.py:38
  214.3 25.7 %copy-start.9 = (f32[4,128]{1,0:T(4,128)S(1)}, f32[4,128]{1,0:T(4,128)}, u32[]{:S(2)}) copy-start(f32[4,128]{1,0:T(4,128)} %get-tuple-element.127) | copy-start | bytes 6148
  250.1 1.0 copy-start.1
  259.1 3.8 copy-start.14
  260.3 2.6 copy-start.2
  261.4 1.5 copy-start.3
  262.9 3.3 copy-start.11
  265.5 60.4 %copy-start.5 = (f32[4,64,4,128]{3,2,1,0:T(4,128)S(1)}, f32[4,64,4,128]{3,2,1,0:T(4,128)}, u32[]{:S(2)}) copy-start(f32[4,64,4,128]{3,2,1,0:T(4,128)} %copy.43) | copy-start | bytes 1572868
  265.5 60.4 %copy-start.13 = (f32[256]{0:T(256)S(1)}, f32[256]{0:T(256)}, u32[]{:S(2)}) copy-start(f32[256]{0:T(256)} %copy-done.12) | copy-start | bytes 3076
  265.5 60.4 %copy-start.16 = (f32[2048]{0:T(1024)S(1)}, f32[2048]{0:T(1024)}, u32[]{:S(2)}) copy-start(f32[2048]{0:T(1024)} %param.19) | copy-start | bytes 24580
Sparse Core Ops, SparseCore 0:
  8.9 11.7 all-gather.26
  22.2 46.8 all-gather.16
  70.7 44.4 all-gather.22
  116.6 44.4 all-gather.14
  162.5 44.4 all-gather.12
  208.4 52.9 all-gather.18
  264.1 61.7 all-gather.20
  328.6 61.1 all-gather.24
  393.2 6.5 reduce-scatter.1
where the time goes:
time: 407 us; the launch traced here: 406 us
  waiting for transfers between devices  252 us (62%)
  blocking collectives  90.1 us (22%)
  matrix products  24 us (6%)
  other arithmetic  13.8 us (3%)
  between operations  13.7 us (3%)
  local copies, waits for them, and re-layouts  9.22 us (2%)
    all_gather x1, waiting for transfers between devices, body(): lax.all_gather(w_out_pool, ('sp', 'fs'), axis=1, tiled=True)  59.8 us
    all_gather x1, waiting for transfers between devices, body(): lax.all_gather(recurrent_output_weight, ('sp', 'fs'), axis=1, tiled=True)  59.5 us
    all_gather x1, waiting for transfers between devices, body(): lax.all_gather(near_rows[2], 'sp', axis=0, tiled=True)  42.4 us
    all_gather x1, waiting for transfers between devices, body(): lax.all_gather(near_rows[4], 'sp', axis=0, tiled=True)  40.8 us
    all_gather x1, waiting for transfers between devices, body(): lax.all_gather(near_rows[0], 'sp', axis=0, tiled=True)  39 us
    all_gather x2, blocking collectives, carried_in(): lax.all_gather(a.astype(kind), axis)  32 us
    all_gather x1, blocking collectives, body(): lax.all_gather(forget_weight, 'fs', axis=0, tiled=True)  13.2 us
    all_gather x1, blocking collectives, body(): lax.all_gather(w_pool, 'fs', axis=0, tiled=True)  11.4 us
  transfers between devices with their start and end apart: 10, of which 7 were waited for; matrix products, arithmetic and copies ran while one was open for 11% of the time, Pallas kernels for 0%

commit v1 on v0

--- a/solution.py
+++ b/solution.py
@@ -165,7 +165,7 @@
     mapped = jnp.einsum("tcd,cde->tce", pooled, local_weight, preferred_element_type=jnp.float32)
     pool_out = (mapped.reshape(tok_rows, pool_dev) * pool_gain).astype(jnp.bfloat16)
     rec_columns, pool_columns = (
-        lax.all_gather(recurrent_output_weight, ("sp", "fs"), axis=1, tiled=True),
+        jnp.concatenate(lax.all_gather(recurrent_output_weight, ("sp", "fs")), axis=1),
         lax.all_gather(w_out_pool, ("sp", "fs"), axis=1, tiled=True),
     )
     mixed = lax.psum_scatter(

time: 407 us -> 398 us (0.978)
  waiting for transfers between devices: 252 us -> 245 us
  blocking collectives: 90.1 us -> 84.3 us
    all_gather x1, waiting for transfers between devices: 59.5 us -> 9.24 us  [body(): lax.all_gather(recurrent_output_weight, ('sp', 'fs'))]
    all_gather x1, waiting for transfers between devices: 0.02 us -> 42 us  [body(): lax.all_gather(near_rows[3], 'sp', axis=0, tiled=True)]
    all_gather x2, blocking collectives: 32 us -> 26.2 us  [carried_in(): lax.all_gather(a.astype(kind), axis)]
  transfers between devices with their start and end apart: 10 -> 10, of which waited for: 7 -> 8; matrix products, arithmetic and copies ran while one was open for 11% -> 12% of each run, Pallas kernels for 0% -> 0%
where the time goes in v1:
time: 398 us; the launch traced here: 397 us
  waiting for transfers between devices  245 us (62%)
  blocking collectives  84.3 us (21%)
  matrix products  24 us (6%)
  other arithmetic  13.8 us (3%)
  between operations  13.6 us (3%)
  local copies, waits for them, and re-layouts  13.2 us (3%)
    all_gather x1, waiting for transfers between devices, body(): lax.all_gather(w_out_pool, ('sp', 'fs'), axis=1, tiled=True)  60.5 us
    all_gather x1, waiting for transfers between devices, body(): lax.all_gather(near_rows[2], 'sp', axis=0, tiled=True)  42.4 us
    all_gather x1, waiting for transfers between devices, body(): lax.all_gather(near_rows[3], 'sp', axis=0, tiled=True)  42 us
    all_gather x1, waiting for transfers between devices, body(): lax.all_gather(near_rows[4], 'sp', axis=0, tiled=True)  40.8 us
    all_gather x1, waiting for transfers between devices, body(): lax.all_gather(near_rows[0], 'sp', axis=0, tiled=True)  39 us
    all_gather x2, blocking collectives, carried_in(): lax.all_gather(a.astype(kind), axis)  26.2 us
    all_gather x1, blocking collectives, body(): lax.all_gather(forget_weight, 'fs', axis=0, tiled=True)  13.2 us
    all_gather x1, blocking collectives, body(): lax.all_gather(w_pool, 'fs', axis=0, tiled=True)  11.4 us
  transfers between devices with their start and end apart: 10, of which 8 were waited for; matrix products, arithmetic and copies ran while one was open for 12% of the time, Pallas kernels for 0%

profile of v1, /device:TPU:0, one launch (start us, length us, event | category | flops | bytes accessed | tf_op | source)
XLA Modules:
  0.0 396.8 jit_solution(11256586523641989647)
XLA Ops:
  6.5 0.7 all-gather.26.cloned.1.call-update
  7.3 13.2 %all_gather.57 = bf16[512,512]{1,0:T(8,128)(2,1)} all-gather(bf16[128,512]{1,0:T(8,128)(2,1)} %param.21), channel_id=1, replica_groups=mesh['sp'=4,'fs'=4,'tp'=2] {'fs'}, dimensions={0}, use_global_device_ids=true | all-gather | bytes 655360 | tf_op jit(solution)/shard_map/all_gather | solution.py:105
  20.6 11.4 %all_gather.66 = bf16[512,512]{1,0:T(8,128)(2,1)} all-gather(bf16[128,512]{1,0:T(8,128)(2,1)} %param.24), channel_id=1, replica_groups=mesh['sp'=4,'fs'=4,'tp'=2] {'fs'}, dimensions={0}, use_global_device_ids=true | all-gather | bytes 655360 | tf_op jit(solution)/shard_map/all_gather | solution.py:108
  32.1 10.5 %all_gather.55 = bf16[512,512]{1,0:T(8,128)(2,1)} all-gather(bf16[128,512]{1,0:T(8,128)(2,1)S(1)} %copy-done.6), channel_id=1, replica_groups=mesh['sp'=4,'fs'=4,'tp'=2] {'fs'}, dimensions={0}, use_global_device_ids=true | all-gather | bytes 655360 | tf_op jit(solution)/shard_map/all_gather | solution.py:104
  42.7 10.4 %all_gather.53 = bf16[512,512]{1,0:T(8,128)(2,1)} all-gather(bf16[128,512]{1,0:T(8,128)(2,1)S(1)} %copy-done.7), channel_id=1, replica_groups=mesh['sp'=4,'fs'=4,'tp'=2] {'fs'}, dimensions={0}, use_global_device_ids=true | all-gather | bytes 655360 | tf_op jit(solution)/shard_map/all_gather | solution.py:106
  53.7 10.1 %all_gather.62 = bf16[512,512]{1,0:T(8,128)(2,1)} all-gather(bf16[128,512]{1,0:T(8,128)(2,1)S(1)} %copy-done.8), channel_id=1, replica_groups=mesh['sp'=4,'fs'=4,'tp'=2] {'fs'}, dimensions={0}, use_global_device_ids=true | all-gather | bytes 655360 | tf_op jit(solution)/shard_map/all_gather | solution.py:107
  63.8 0.7 all-gather.24.cloned.1.call-update
  65.5 1.5 fusion.1
  67.1 2.0 all-gather.18.cloned.1.call-done
  69.1 2.9 negate_log-plus-one_fusion
  72.6 1.2 slice_bitcast_fusion
  73.7 0.6 fusion.15
  74.4 40.8 %all-gather.22.cloned.1.call-done = bf16[2048,512]{1,0:T(8,128)(2,1)} async-done(((bf16[512,512]{1,0:T(8,128)(2,1)}), bf16[2048,512]{1,0:T(8,128)(2,1)}) %all-gather.22.cloned.1.call-update) | async-done | bytes 2097168 | tf_op jit(solution)/shard_map/all_gather | solution.py:115
  115.2 2.7 convolution_convert_fusion
  117.9 0.6 slice.57
  118.5 2.7 collective-permute-start
  121.1 1.0 reshape_reshape.11
  122.1 39.0 %all-gather.16.cloned.1.call-done = bf16[2048,512]{1,0:T(8,128)(2,1)} async-done(((bf16[512,512]{1,0:T(8,128)(2,1)}), bf16[2048,512]{1,0:T(8,128)(2,1)}) %all-gather.16.cloned.1.call-update) | async-done | bytes 2097168 | tf_op jit(solution)/shard_map/all_gather | solution.py:111
  161.1 2.4 divide_multiply_fusion
  163.5 1.0 reshape_reshape.10
  164.6 42.4 %all-gather.14.cloned.1.call-done = bf16[2048,512]{1,0:T(8,128)(2,1)} async-done(((bf16[512,512]{1,0:T(8,128)(2,1)}), bf16[2048,512]{1,0:T(8,128)(2,1)}) %all-gather.14.cloned.1.call-update) | async-done | bytes 2097168 | tf_op jit(solution)/shard_map/all_gather | solution.py:113
  207.0 2.3 convolution_convert_fusion.4
  209.4 1.7 exponential_multiply_fusion.1
  211.1 1.0 convolution_select_fusion
  212.1 1.2 fusion.39
  213.3 1.0 fusion.21
  214.3 3.7 while.26
  214.3 0.7 bitcast_dynamic-update-slice_fusion.2
  215.2 0.7 bitcast_dynamic-update-slice_fusion.2
  216.2 0.7 bitcast_dynamic-update-slice_fusion.2
  217.1 0.7 bitcast_dynamic-update-slice_fusion.2
  218.0 16.4 %all-gather.2 = bf16[16,128,128]{2,1,0:T(8,128)(2,1)S(1)} all-gather(bf16[4,128,128]{2,1,0:T(8,128)(2,1)S(1)} %convert_element_type.97), channel_id=4, replica_groups=mesh['sp'=4,'fs'=4,'tp'=2] {'sp'}, dimensions={0}, use_global_device_ids=true | all-gather | bytes 655360 | tf_op jit(solution)/shard_map/all_gather | solution.py:18
  234.5 9.7 %all-gather.4 = bf16[4,4,128]{2,1,0:T(4,128)(2,1)S(1)} all-gather(bf16[1,4,128]{2,1,0:T(4,128)(2,1)S(1)} %fusion.42), channel_id=3, replica_groups=mesh['sp'=4,'fs'=4,'tp'=2] {'sp'}, dimensions={0}, use_global_device_ids=true | all-gather | bytes 5120 | tf_op jit(solution)/shard_map/all_gather | solution.py:18
  245.2 2.3 multiply_reduce_fusion
  247.7 2.6 psum.7
  250.6 1.1 copy.67
  251.8 0.8 maximum_convert_fusion
  253.2 1.1 stack.18
  254.4 1.1 stack.17
  255.5 1.1 stack.16
  257.0 2.6 fusion.4
  260.4 9.2 %all-gather.28.cloned.1.call-done = bf16[8192,128]{1,0:T(8,128)(2,1)} async-done(((bf16[512,128]{1,0:T(8,128)(2,1)}), bf16[8192,128]{1,0:T(8,128)(2,1)}) %all-gather.28.cloned.1.call-update) | async-done | bytes 2097168 | tf_op jit(solution)/shard_map/all_gather | solution.py:168
  269.7 4.0 %copy.68 = bf16[512,16,128]{0,2,1:T(8,128)(2,1)} copy(bf16[512,16,128]{2,0,1:T(8,128)(2,1)} %bitcast.87) | data formatting | bytes 4194304 | tf_op jit(solution)/shard_map/reshape | solution.py:168
  273.7 42.0 %all-gather.20.cloned.1.call-done = bf16[2048,512]{1,0:T(8,128)(2,1)} async-done(((bf16[512,512]{1,0:T(8,128)(2,1)}), bf16[2048,512]{1,0:T(8,128)(2,1)}) %all-gather.20.cloned.1.call-update) | async-done | bytes 2097168 | tf_op jit(solution)/shard_map/all_gather | solution.py:114
  315.8 4.0 %fusion.24 = f32[256,2048]{1,0:T(8,128)S(1)} fusion(bf16[512,2048]{0,1:T(8,128)(2,1)} %bitcast.88, f32[32,8,4,128]{3,2,1,0:T(4,128)S(1)} %bitcast.90, bf16[2048,512]{1,0:T(8,128)(2,1)} %all-gather.20.cloned.1.call-done, f32[512]{0:T(512)S(1)} %copy-done.18, f32[256]{0:T(256)S(1)} %add_rsqrt_fusion, bf16[1,256,2048]{2,1,0:T(8,128)(2,1)} %all-gather.26.cloned.1.call-done, ...), kind=kOutput, calls=%fused_computation.49 | convolution fusion | flops 1077149696 | bytes 7876608 | tf_op jit(solution)/shard_map/dot_general | solution.py:173
  319.8 60.5 %all-gather.24.cloned.1.call-done = bf16[512,2048]{1,0:T(8,128)(2,1)} async-done(((bf16[512,128]{1,0:T(8,128)(2,1)}), bf16[512,2048]{1,0:T(8,128)(2,1)}) %all-gather.24.cloned.1.call-update) | async-done | bytes 2097168 | tf_op jit(solution)/shard_map/all_gather | solution.py:169
  380.2 3.3 fusion
  383.6 6.7 %reduce-scatter.2.cloned.1.call-done = bf16[128,2048]{1,0:T(8,128)(2,1)} async-done(((bf16[256,2048]{1,0:T(8,128)(2,1)}), bf16[128,2048]{1,0:T(8,128)(2,1)}) %reduce-scatter.2.cloned.1.call-update) | async-done | bytes 524304 | tf_op jit(solution)/shard_map/reduce_scatter | solution.py:171
  (98 shorter events, 6.4 us)
Async XLA Ops:
  6.5 253.5 %copy-start = (bf16[4,256,256]{2,1,0:T(8,128)(2,1)S(1)}, bf16[4,256,256]{2,1,0:T(8,128)(2,1)}, u32[]{:S(2)}) copy-start(bf16[4,256,256]{2,1,0:T(8,128)(2,1)} %param.28) | copy-start | bytes 1572868
  6.5 25.5 %copy-start.6 = (bf16[128,512]{1,0:T(8,128)(2,1)S(1)}, bf16[128,512]{1,0:T(8,128)(2,1)}, u32[]{:S(2)}) copy-start(bf16[128,512]{1,0:T(8,128)(2,1)} %param.20) | copy-start | bytes 393220
  6.5 36.1 %copy-start.7 = (bf16[128,512]{1,0:T(8,128)(2,1)S(1)}, bf16[128,512]{1,0:T(8,128)(2,1)}, u32[]{:S(2)}) copy-start(bf16[128,512]{1,0:T(8,128)(2,1)} %param.22) | copy-start | bytes 393220
  6.5 59.0 %all-gather.26.cloned.1.call-start = ((), (), s32[]{:S(2)}) async-start(), calls=%async_computation.8 | async-start | bytes 1572864 | tf_op jit(solution)/shard_map/all_gather | solution.py:96
  7.3 61.8 %all-gather.18.cloned.1.call-start = ((), (), s32[]{:S(2)}) async-start(), calls=%async_computation.3 | async-start | bytes 2621440 | tf_op jit(solution)/shard_map/all_gather | solution.py:112
  20.5 33.2 %copy-start.8 = (bf16[128,512]{1,0:T(8,128)(2,1)S(1)}, bf16[128,512]{1,0:T(8,128)(2,1)}, u32[]{:S(2)}) copy-start(bf16[128,512]{1,0:T(8,128)(2,1)} %param.23) | copy-start | bytes 393220
  20.5 94.7 %all-gather.22.cloned.1.call-start = ((), (), s32[]{:S(2)}) async-start(), calls=%async_computation.5 | async-start | bytes 2621440 | tf_op jit(solution)/shard_map/all_gather | solution.py:115
  32.0 33.4 %copy-start.10 = (f32[1,256,4]{1,2,0:T(4,128)S(1)}, f32[1,256,4]{1,2,0:T(4,128)}, u32[]{:S(2)}) copy-start(f32[1,256,4]{1,2,0:T(4,128)} %param.26) | copy-start | bytes 12292
  32.0 129.1 %all-gather.16.cloned.1.call-start = ((), (), s32[]{:S(2)}) async-start(), calls=%async_computation.2 | async-start | bytes 2621440 | tf_op jit(solution)/shard_map/all_gather | solution.py:111
  42.6 26.5 %copy-start.15 = (f32[2048]{0:T(1024)S(1)}, f32[2048]{0:T(1024)}, u32[]{:S(2)}) copy-start(f32[2048]{0:T(1024)} %param.19) | copy-start | bytes 24580
  42.6 26.5 %copy-start.17 = (f32[512]{0:T(512)S(1)}, f32[512]{0:T(512)}, u32[]{:S(2)}) copy-start(f32[512]{0:T(512)} %param.25) | copy-start | bytes 6148
  42.6 164.4 %all-gather.14.cloned.1.call-start = ((), (), s32[]{:S(2)}) async-start(), calls=%async_computation.1 | async-start | bytes 2621440 | tf_op jit(solution)/shard_map/all_gather | solution.py:113
  53.0 216.6 %all-gather.28.cloned.1.call-start = ((), (), s32[]{:S(2)}) async-start(), calls=%async_computation.9 | async-start | bytes 2228224 | tf_op jit(solution)/shard_map/all_gather | solution.py:168
  53.6 262.1 %all-gather.20.cloned.1.call-start = ((), (), s32[]{:S(2)}) async-start(), calls=%async_computation.4 | async-start | bytes 2621440 | tf_op jit(solution)/shard_map/all_gather | solution.py:114
  63.8 316.4 %all-gather.24.cloned.1.call-start = ((), (), s32[]{:S(2)}) async-start(), calls=%async_computation.6 | async-start | bytes 2228224 | tf_op jit(solution)/shard_map/all_gather | solution.py:169
  64.5 325.8 %reduce-scatter.2.cloned.1.call-start = ((), (), s32[]{:S(2)}) async-start(), calls=%async_computation.7 | async-start | bytes 1572864 | tf_op jit(solution)/shard_map/reduce_scatter | solution.py:171
  67.1 139.9 %copy-start.12 = (f32[256]{0:T(256)}, f32[256]{0:T(256)S(1)}, u32[]{:S(2)}) copy-start(f32[256]{0:T(256)S(1)} %add_rsqrt_fusion.1) | copy-start | bytes 3076
  74.4 86.7 %copy-start.4 = (bf16[1,256,2048]{2,1,0:T(8,128)(2,1)S(1)}, bf16[1,256,2048]{2,1,0:T(8,128)(2,1)}, u32[]{:S(2)}) copy-start(bf16[1,256,2048]{2,1,0:T(8,128)(2,1)} %all-gather.26.cloned.1.call-done) | copy-start | bytes 3145732
  118.5 133.3 %collective-permute-start = (bf16[16,512]{1,0:T(8,128)(2,1)}, bf16[16,512]{1,0:T(8,128)(2,1)}, u32[]{:S(2)}, u32[]{:S(2)}) collective-permute-start(bf16[16,512]{1,0:T(8,128)(2,1)} %slice.57), channel_id=1, source_target_pairs={{0,8},{8,16},{16,24},{1,9},{9,17},{17,25},{2,10},{10,18},{18,26},{... | collective-permute-start | bytes 49160 | tf_op jit(solution)/shard_map/ppermute | solution.py:38
  214.3 20.2 %copy-start.9 = (f32[4,128]{1,0:T(4,128)S(1)}, f32[4,128]{1,0:T(4,128)}, u32[]{:S(2)}) copy-start(f32[4,128]{1,0:T(4,128)} %get-tuple-element.127) | copy-start | bytes 6148
  244.2 1.0 copy-start.1
  253.2 3.7 copy-start.14
  254.4 2.6 copy-start.2
  255.5 1.5 copy-start.3
  257.0 3.3 copy-start.11
  269.7 46.1 %copy-start.5 = (f32[4,64,4,128]{3,2,1,0:T(4,128)S(1)}, f32[4,64,4,128]{3,2,1,0:T(4,128)}, u32[]{:S(2)}) copy-start(f32[4,64,4,128]{3,2,1,0:T(4,128)} %copy.67) | copy-start | bytes 1572868
  269.7 46.1 %copy-start.13 = (f32[256]{0:T(256)S(1)}, f32[256]{0:T(256)}, u32[]{:S(2)}) copy-start(f32[256]{0:T(256)} %copy-done.12) | copy-start | bytes 3076
  269.7 46.1 %copy-start.16 = (f32[2048]{0:T(1024)S(1)}, f32[2048]{0:T(1024)}, u32[]{:S(2)}) copy-start(f32[2048]{0:T(1024)} %param.19) | copy-start | bytes 24580
  269.7 46.1 %copy-start.18 = (f32[512]{0:T(512)S(1)}, f32[512]{0:T(512)}, u32[]{:S(2)}) copy-start(f32[512]{0:T(512)} %param.27) | copy-start | bytes 6148
Sparse Core Ops, SparseCore 0:
  8.9 11.7 all-gather.25
  22.2 46.8 all-gather.17
  70.7 44.4 all-gather.21
  116.6 44.4 all-gather.15
  162.5 44.4 all-gather.13
  209.6 60.0 all-gather.27
  271.3 44.4 all-gather.19
  318.4 61.7 all-gather.23
  383.7 6.5 reduce-scatter.1
